TPU v7x, 512 devices: a whole 4x4x16 slice. The times are simulated.
512 devices in a mesh: ra: 16 (over z), cb: 4 (over y), dp: 8 (over x, core).
Axes of the slice: x: 4, y: 4, z: 16, core: 2. Of those that a mesh axis runs over, the one named last changes fastest.
Arguments:
- tokens: bfloat16 [8, 512, 4096], P('dp', None, 'ra'), may hold values from -80 to 80
- pre_gain: float32 [4096], P('ra'), may hold values from 0.1 to 1.9
- w_gate: bfloat16 [4096, 11264], P('ra', 'cb'), may hold values from -0.09375 to 0.09375
- w_up: bfloat16 [4096, 11264], P('ra', 'cb'), may hold values from -0.09375 to 0.09375
- conv_gate: float32 [3, 11264], P(None, 'cb'), may hold values from -3.5 to 3.5
- conv_up: float32 [3, 11264], P(None, 'cb'), may hold values from -3.5 to 3.5
- w_down: bfloat16 [11264, 4096], P('cb', 'ra'), may hold values from -2 to 2
- post_gain: float32 [4096], P('ra'), may hold values from 0.1 to 1.9
Outputs:
- mixed: bfloat16 [8, 512, 4096], P('dp', None, 'ra')
All inputs are finite; a program needn't handle non-finite values.
Results may differ from a plain program's by a relative error of at most 0.0064.
Values may be sent and summed in bfloat16 or wider, within the bound.
A program may use at most 64 MiB of HBM per device.

v0:
```python
import jax
import jax.numpy as jnp
from jax import lax
from jax.sharding import PartitionSpec as P

epsilon = 1e-06
residual_scale = 0.125


def from_everyone(array, axis):
    count = lax.axis_size(axis)
    return lax.all_to_all(
        jnp.broadcast_to(array[None], (count, *array.shape)), axis, 0, 0, tiled=True
    )


def over_copies(array, axis):
    return from_everyone(array, axis).sum(axis=0)


def split_up(array, dim, count):
    dims = array.shape
    tiles = array.reshape(*dims[:dim], count, dims[dim] // count, *dims[dim + 1 :])
    return jnp.moveaxis(tiles, dim, 0)


def summed_on_arrival(array, axis, dim):
    count = lax.axis_size(axis)
    tiles = lax.all_to_all(split_up(array, dim, count), axis, 0, 0, tiled=True)
    return jnp.sum(tiles, axis=0)


def convolve(field, tap_weights):
    zero_col = jnp.zeros((field.shape[0], 1), jnp.float32)
    before = jnp.concatenate([zero_col, field[:, :-1]], axis=1)
    later_cols = jnp.concatenate([field[:, 1:], zero_col], axis=1)
    return (
        tap_weights[0][:, None] * before
        + tap_weights[1][:, None] * field
        + tap_weights[2][:, None] * later_cols
    )


def local(tokens, pre_gain, w_gate, w_up, conv_gate, conv_up, w_down, post_gain):
    ra_count = lax.axis_size("ra")
    dim_full = tokens.shape[2] * ra_count
    values = tokens[0].astype(jnp.float32)
    local_sq = jnp.sum(values * values, axis=1)
    total_sq = over_copies(local_sq, "ra")
    in_scale = lax.rsqrt(total_sq / dim_full + epsilon)
    weighted = (values * pre_gain).astype(jnp.bfloat16)
    gate_cols, up_cols = (
        lax.all_to_all(w_gate, "ra", split_axis=1, concat_axis=0, tiled=True),
        lax.all_to_all(w_up, "ra", split_axis=1, concat_axis=0, tiled=True),
    )
    own_units = gate_cols.shape[1]
    piece = lax.all_gather(weighted, "ra", axis=1, tiled=True)
    dims = (((0,), (1,)), ((), ()))
    gate_sum = lax.dot_general(gate_cols, piece, dims, preferred_element_type=jnp.float32)
    up_sum = lax.dot_general(up_cols, piece, dims, preferred_element_type=jnp.float32)
    offset_units = lax.axis_index("ra") * own_units
    taps_gate = lax.dynamic_slice_in_dim(conv_gate, offset_units, own_units, 1)
    taps_up = lax.dynamic_slice_in_dim(conv_up, offset_units, own_units, 1)
    gate_lin = gate_sum * in_scale[None, :]
    up_lin = up_sum * in_scale[None, :]
    hidden = (
        jax.nn.gelu(convolve(gate_lin, taps_gate), approximate=True) * convolve(up_lin, taps_up)
    ).astype(jnp.bfloat16)
    partial_value = lax.dot_general(
        lax.all_gather(hidden, "ra", axis=0, tiled=True),
        w_down,
        (((0,), (0,)), ((), ())),
        preferred_element_type=jnp.float32,
    )
    share = summed_on_arrival(partial_value, "cb", 1)
    share_cols = share.shape[1]
    col_start = lax.axis_index("cb") * share_cols
    own_values = lax.dynamic_slice_in_dim(values, col_start, share_cols, 1)
    own_gain = lax.dynamic_slice_in_dim(post_gain, col_start, share_cols, 0)
    post_sq = over_copies(jnp.sum(share * share, axis=1), ("ra", "cb"))
    post_scale = lax.rsqrt(post_sq / dim_full + epsilon)
    mixed_part = (residual_scale * own_values + share * post_scale[:, None] * own_gain).astype(
        jnp.bfloat16
    )
    mixed = lax.all_gather(mixed_part, "cb", axis=1, tiled=True)
    return mixed[None]


def solution(mesh):
    in_specs = (
        P("dp", None, "ra"),
        P("ra"),
        P("ra", "cb"),
        P("ra", "cb"),
        P(None, "cb"),
        P(None, "cb"),
        P("cb", "ra"),
        P("ra"),
    )
    out_specs = P("dp", None, "ra")
    return jax.shard_map(local, mesh=mesh, in_specs=in_specs, out_specs=out_specs, check_vma=False)
```

profile of v0, /device:TPU:2, one launch (start us, length us, event | category | flops | bytes accessed | tf_op | source)
XLA Modules:
  0.0 356.9 jit_solution(16461781965745227600)
XLA Ops:
  6.5 0.0 copy-start
  6.5 1.2 copy.25
  7.7 1.5 fusion.3
  9.2 0.6 broadcast_in_dim.6
  9.9 15.2 %all-to-all-start.1 = ((f32[16,1,512]{2,1,0:T(1,128)}), f32[16,1,512]{2,1,0:T(1,128)S(1)}, u32[]{:S(2)}, u32[]{:S(2)}) async-start(f32[16,1,512]{2,1,0:T(1,128)} %broadcast_in_dim.6), calls=%async_computation.1 | async-start | bytes 65536 | tf_op jit(solution)/shard_map/all_to_all | solution.py:12
  25.1 2.5 copy.29
  27.6 10.0 %all-to-all-done.1 = f32[16,1,512]{2,1,0:T(1,128)S(1)} async-done(((f32[16,1,512]{2,1,0:T(1,128)}), f32[16,1,512]{2,1,0:T(1,128)S(1)}, u32[]{:S(2)}, u32[]{:S(2)}) %all-to-all-start.1) | async-done | bytes 32800 | tf_op jit(solution)/shard_map/all_to_all | solution.py:12
  37.6 3.7 %all-to-all-start.2 = ((bf16[256,16,176]{0,2,1:T(8,128)(2,1)}), bf16[256,16,176]{0,2,1:T(8,128)(2,1)S(1)}, u32[]{:S(2)}, u32[]{:S(2)}) async-start(bf16[256,16,176]{0,2,1:T(8,128)(2,1)} %bitcast.41), calls=%async_computation.2 | async-start | bytes 2883584 | tf_op jit(solution)/shard_map/all_to_all | solution.py:54
  41.3 0.0 all-gather.3.cloned.1.call-start
  41.4 0.7 all-gather.3.cloned.1.call-update
  42.1 2.5 copy.26
  44.6 72.1 %all-to-all-done.2 = bf16[256,16,176]{0,2,1:T(8,128)(2,1)S(1)} async-done(((bf16[256,16,176]{0,2,1:T(8,128)(2,1)}), bf16[256,16,176]{0,2,1:T(8,128)(2,1)S(1)}, u32[]{:S(2)}, u32[]{:S(2)}) %all-to-all-start.2) | async-done | bytes 1441824 | tf_op jit(solution)/shard_map/all_to_all | solution.py:54
  116.7 10.3 %all-to-all-start = ((bf16[256,16,176]{0,2,1:T(8,128)(2,1)}), bf16[256,16,176]{0,2,1:T(8,128)(2,1)}, u32[]{:S(2)}, u32[]{:S(2)}) async-start(bf16[256,16,176]{0,2,1:T(8,128)(2,1)} %bitcast.40), calls=%async_computation | async-start | bytes 2883584 | tf_op jit(solution)/shard_map/all_to_all | solution.py:53
  127.0 0.0 all-gather.5.cloned.1.call-start
  127.1 0.9 constant_dynamic-slice_fusion
  128.0 1.3 copy.36
  129.3 78.8 %all-to-all-done = bf16[256,16,176]{0,2,1:T(8,128)(2,1)} async-done(((bf16[256,16,176]{0,2,1:T(8,128)(2,1)}), bf16[256,16,176]{0,2,1:T(8,128)(2,1)}, u32[]{:S(2)}, u32[]{:S(2)}) %all-to-all-start) | async-done | bytes 1441824 | tf_op jit(solution)/shard_map/all_to_all | solution.py:53
  208.2 0.0 copy-start.2
  208.2 2.8 copy.35
  210.9 5.6 %all-gather.3.cloned.1.call-done = bf16[512,4096]{0,1:T(8,128)(2,1)} async-done(((bf16[512,256]{0,1:T(8,128)(2,1)}), bf16[512,4096]{0,1:T(8,128)(2,1)}) %all-gather.3.cloned.1.call-update) | async-done | bytes 4194320 | tf_op jit(solution)/shard_map/all_gather | solution.py:57
  216.5 0.0 copy-done.2
  216.5 0.0 copy-start.1
  216.5 0.0 copy-start.3
  216.5 3.3 fusion.1
  219.8 0.2 copy-done.1
  220.0 0.4 copy-done.3
  220.4 0.9 fusion
  221.3 0.3 fusion.14
  221.6 1.2 fusion.12
  222.8 0.0 all-gather.5.cloned.1.call-update
  222.8 72.5 %all-gather.5.cloned.1.call-done = bf16[2816,512]{1,0:T(8,128)(2,1)} async-done(((bf16[176,512]{1,0:T(8,128)(2,1)}), bf16[2816,512]{1,0:T(8,128)(2,1)}) %all-gather.5.cloned.1.call-update) | async-done | bytes 2883600 | tf_op jit(solution)/shard_map/all_gather | solution.py:70
  295.4 0.0 copy-done
  295.4 2.8 fusion.16
  298.1 0.0 copy-start.4
  298.1 12.2 %all_to_all.55 = f32[4,512,64]{1,2,0:T(8,128)S(1)} all-to-all(f32[4,512,64]{1,2,0:T(8,128)S(1)} %bitcast.45), channel_id=1, replica_groups=mesh['ra'=16,'cb'=4,'dp'=8] {'cb'}, dimensions={0} | all-to-all | bytes 1048576 | tf_op jit(solution)/shard_map/all_to_all | solution.py:29
  310.4 0.7 broadcast_in_dim.7
  311.2 9.4 %all-to-all-start.4 = ((f32[64,1,512]{2,1,0:T(1,128)}), f32[64,1,512]{2,1,0:T(1,128)S(1)}, u32[]{:S(2)}, u32[]{:S(2)}) async-start(f32[64,1,512]{2,1,0:T(1,128)} %broadcast_in_dim.7), calls=%async_computation.4 | async-start | bytes 262144 | tf_op jit(solution)/shard_map/all_to_all | solution.py:12
  320.6 0.1 convert_element_type.15
  320.6 0.0 copy-done.4
  320.7 0.1 dynamic_slice.15
  320.7 16.0 %all-to-all-done.4 = f32[64,1,512]{2,1,0:T(1,128)S(1)} async-done(((f32[64,1,512]{2,1,0:T(1,128)}), f32[64,1,512]{2,1,0:T(1,128)S(1)}, u32[]{:S(2)}, u32[]{:S(2)}) %all-to-all-start.4) | async-done | bytes 131104 | tf_op jit(solution)/shard_map/all_to_all | solution.py:12
  336.7 0.1 reduce_sum.49
  336.8 0.1 fusion.13
  336.9 12.3 %all_gather.11 = bf16[512,256]{0,1:T(8,128)(2,1)S(1)} all-gather(bf16[512,64]{0,1:T(8,128)(2,1)S(1)} %fusion.13), channel_id=1, replica_groups=mesh['ra'=16,'cb'=4,'dp'=8] {'cb'}, dimensions={1}, use_global_device_ids=true | all-gather | bytes 327680 | tf_op jit(solution)/shard_map/all_gather | solution.py:85
  349.2 0.8 copy.32
  (5 shorter events, 0.1 us)
Async XLA Ops:
  6.5 288.8 %copy-start = (bf16[2816,256]{1,0:T(8,128)(2,1)S(1)}, bf16[2816,256]{1,0:T(8,128)(2,1)}, u32[]{:S(2)}) copy-start(bf16[2816,256]{1,0:T(8,128)(2,1)} %param.14) | copy-start | bytes 4325380
  9.9 27.8 %all-to-all-start.1 = ((f32[16,1,512]{2,1,0:T(1,128)}), f32[16,1,512]{2,1,0:T(1,128)S(1)}, u32[]{:S(2)}, u32[]{:S(2)}) async-start(f32[16,1,512]{2,1,0:T(1,128)} %broadcast_in_dim.6), calls=%async_computation.1 | async-start | bytes 65536 | tf_op jit(solution)/shard_map/all_to_all | solution.py:12
  37.6 79.1 %all-to-all-start.2 = ((bf16[256,16,176]{0,2,1:T(8,128)(2,1)}), bf16[256,16,176]{0,2,1:T(8,128)(2,1)S(1)}, u32[]{:S(2)}, u32[]{:S(2)}) async-start(bf16[256,16,176]{0,2,1:T(8,128)(2,1)} %bitcast.41), calls=%async_computation.2 | async-start | bytes 2883584 | tf_op jit(solution)/shard_map/all_to_all | solution.py:54
  41.3 175.2 %all-gather.3.cloned.1.call-start = ((), (), s32[]{:S(2)}) async-start(), calls=%async_computation.5 | async-start | bytes 4456448 | tf_op jit(solution)/shard_map/all_gather | solution.py:57
  116.7 91.4 %all-to-all-start = ((bf16[256,16,176]{0,2,1:T(8,128)(2,1)}), bf16[256,16,176]{0,2,1:T(8,128)(2,1)}, u32[]{:S(2)}, u32[]{:S(2)}) async-start(bf16[256,16,176]{0,2,1:T(8,128)(2,1)} %bitcast.40), calls=%async_computation | async-start | bytes 2883584 | tf_op jit(solution)/shard_map/all_to_all | solution.py:53
  127.0 168.3 %all-gather.5.cloned.1.call-start = ((), (), s32[]{:S(2)}) async-start(), calls=%async_computation.6 | async-start | bytes 3063808 | tf_op jit(solution)/shard_map/all_gather | solution.py:70
  208.2 8.4 %copy-start.2 = (bf16[16,22,8,256]{3,2,0,1:T(8,128)(2,1)S(1)}, bf16[16,22,8,256]{3,2,0,1:T(8,128)(2,1)}, u32[]{:S(2)}) copy-start(bf16[16,22,8,256]{3,2,0,1:T(8,128)(2,1)} %copy.36) | copy-start | bytes 4325380
  216.5 3.4 copy-start.1
  216.5 3.9 %copy-start.3 = (bf16[16,22,8,256]{3,2,0,1:T(8,128)(2,1)S(1)}, bf16[16,22,8,256]{3,2,0,1:T(8,128)(2,1)}, u32[]{:S(2)}) copy-start(bf16[16,22,8,256]{3,2,0,1:T(8,128)(2,1)} %copy.35) | copy-start | bytes 4325380
  298.1 22.5 %copy-start.4 = (f32[256]{0:T(256)S(1)}, f32[256]{0:T(256)}, u32[]{:S(2)}) copy-start(f32[256]{0:T(256)} %param.15) | copy-start | bytes 3076
  311.2 25.6 %all-to-all-start.4 = ((f32[64,1,512]{2,1,0:T(1,128)}), f32[64,1,512]{2,1,0:T(1,128)S(1)}, u32[]{:S(2)}, u32[]{:S(2)}) async-start(f32[64,1,512]{2,1,0:T(1,128)} %broadcast_in_dim.7), calls=%async_computation.4 | async-start | bytes 262144 | tf_op jit(solution)/shard_map/all_to_all | solution.py:12
Sparse Core Ops, SparseCore 0:
  44.2 172.2 all-gather.2
  222.9 72.3 all-gather.4
where the time goes:
time: 357 us
  waiting for transfers between devices  256 us (72%)
  starting transfers between devices  38.7 us (11%)
  blocking collectives  24.5 us (7%)
  local copies, waits for them, and re-layouts  14.4 us (4%)
  between operations  13.5 us (4%)
  matrix products  6.94 us (2%)
    all_to_all x1, waiting for transfers between devices, local(): lax.all_to_all(w_gate, 'ra', split_axis=1, concat_axis=0, tiled=True)  78.8 us
    all_gather x1, waiting for transfers between devices, local(): lax.all_gather(hidden, 'ra', axis=0, tiled=True)  72.5 us
    all_to_all x1, waiting for transfers between devices, local(): lax.all_to_all(w_up, 'ra', split_axis=1, concat_axis=0, tiled=True)  72.1 us
    all_to_all x2, waiting for transfers between devices, from_everyone(): lax.all_to_all(jnp.broadcast_to(array[None], (count, *array.shape)), axis...  26 us
    all_to_all x2, starting transfers between devices, from_everyone(): lax.all_to_all(jnp.broadcast_to(array[None], (count, *array.shape)), axis...  24.6 us
    all_gather x1, blocking collectives, local(): mixed = lax.all_gather(mixed_part, 'cb', axis=1, tiled=True)  12.3 us
    all_to_all x1, blocking collectives, summed_on_arrival(): tiles = lax.all_to_all(split_up(array, dim, count), axis, 0, 0, tiled=True)  12.2 us
    all_to_all x1, starting transfers between devices, local(): lax.all_to_all(w_gate, 'ra', split_axis=1, concat_axis=0, tiled=True)  10.3 us
  transfers between devices with their start and end apart: 6, of which 6 were waited for; matrix products, arithmetic and copies ran while one was open for 3% of the time, Pallas kernels for 0%

commit v1 on v0

--- a/solution.py
+++ b/solution.py
@@ -67,7 +67,9 @@
         jax.nn.gelu(convolve(gate_lin, taps_gate), approximate=True) * convolve(up_lin, taps_up)
     ).astype(jnp.bfloat16)
     partial_value = lax.dot_general(
-        lax.all_gather(hidden, "ra", axis=0, tiled=True),
+        jnp.concatenate(
+            lax.all_to_all(jnp.stack([hidden] * lax.axis_size("ra")), "ra", 0, 0), axis=0
+        ),
         w_down,
         (((0,), (0,)), ((), ())),
         preferred_element_type=jnp.float32,

time: 357 us -> 421 us (1.18)
  waiting for transfers between devices: 256 us -> 305 us
  starting transfers between devices: 38.7 us -> 50.8 us
    all_to_all x0 -> x1, waiting for transfers between devices: none -> 120 us  [local(): lax.all_to_all(jnp.stack([hidden] * lax.axis_size('ra')), 'ra', 0, 0)]
    all_gather x1 -> x0, waiting for transfers between devices: 72.5 us -> none  [local(): lax.all_gather(hidden, 'ra', axis=0, tiled=True)]
    all_to_all x0 -> x1, starting transfers between devices: none -> 8.62 us  [local(): lax.all_to_all(jnp.stack([hidden] * lax.axis_size('ra')), 'ra', 0, 0)]
  transfers between devices with their start and end apart: 6 -> 6, of which waited for: 6 -> 6; matrix products, arithmetic and copies ran while one was open for 3% -> 2% of each run, Pallas kernels for 0% -> 0%
where the time goes in v1:
time: 421 us; the launch traced here: 420 us
  waiting for transfers between devices  305 us (72%)
  starting transfers between devices  50.8 us (12%)
  blocking collectives  25.3 us (6%)
  local copies, waits for them, and re-layouts  16.3 us (4%)
  between operations  13.6 us (3%)
  matrix products  6.44 us (2%)
    all_to_all x1, waiting for transfers between devices, local(): lax.all_to_all(jnp.stack([hidden] * lax.axis_size('ra')), 'ra', 0, 0)  120 us
    all_to_all x1, waiting for transfers between devices, local(): lax.all_to_all(w_gate, 'ra', split_axis=1, concat_axis=0, tiled=True)  78.8 us
    all_to_all x1, waiting for transfers between devices, local(): lax.all_to_all(w_up, 'ra', split_axis=1, concat_axis=0, tiled=True)  73.1 us
    all_to_all x2, starting transfers between devices, from_everyone(): lax.all_to_all(jnp.broadcast_to(array[None], (count, *array.shape)), axis...  28.1 us
    all_to_all x2, waiting for transfers between devices, from_everyone(): lax.all_to_all(jnp.broadcast_to(array[None], (count, *array.shape)), axis...  26.1 us
    all_to_all x1, blocking collectives, summed_on_arrival(): tiles = lax.all_to_all(split_up(array, dim, count), axis, 0, 0, tiled=True)  13 us
    all_gather x1, blocking collectives, local(): mixed = lax.all_gather(mixed_part, 'cb', axis=1, tiled=True)  12.3 us
    all_to_all x1, starting transfers between devices, local(): lax.all_to_all(w_gate, 'ra', split_axis=1, concat_axis=0, tiled=True)  10.2 us
  transfers between devices with their start and end apart: 6, of which 6 were waited for; matrix products, arithmetic and copies ran while one was open for 2% of the time, Pallas kernels for 0%

profile of v1, /device:TPU:2, one launch (start us, length us, event | category | flops | bytes accessed | tf_op | source)
XLA Modules:
  0.0 420.1 jit_solution(13928984655073143669)
XLA Ops:
  6.5 1.1 copy.29
  7.6 1.5 fusion.3
  9.1 0.6 broadcast_in_dim.6
  9.7 15.2 %all-to-all-start.1 = ((f32[16,1,512]{2,1,0:T(1,128)}), f32[16,1,512]{2,1,0:T(1,128)S(1)}, u32[]{:S(2)}, u32[]{:S(2)}) async-start(f32[16,1,512]{2,1,0:T(1,128)} %broadcast_in_dim.6), calls=%async_computation.1 | async-start | bytes 65536 | tf_op jit(solution)/shard_map/all_to_all | solution.py:12
  25.0 2.6 copy.33
  27.5 10.0 %all-to-all-done.1 = f32[16,1,512]{2,1,0:T(1,128)S(1)} async-done(((f32[16,1,512]{2,1,0:T(1,128)}), f32[16,1,512]{2,1,0:T(1,128)S(1)}, u32[]{:S(2)}, u32[]{:S(2)}) %all-to-all-start.1) | async-done | bytes 32800 | tf_op jit(solution)/shard_map/all_to_all | solution.py:12
  37.5 0.0 copy-start.3
  37.5 3.8 all-to-all-start.2
  41.4 0.0 all-gather.2.cloned.1.call-start
  41.4 0.7 all-gather.2.cloned.1.call-update
  42.1 0.0 copy-done.3
  42.1 1.6 copy.30
  43.7 73.1 %all-to-all-done.2 = bf16[256,16,176]{0,2,1:T(8,128)(2,1)S(1)} async-done(((bf16[256,16,176]{0,2,1:T(8,128)(2,1)}), bf16[256,16,176]{0,2,1:T(8,128)(2,1)S(1)}, u32[]{:S(2)}, u32[]{:S(2)}) %all-to-all-start.2) | async-done | bytes 1441824 | tf_op jit(solution)/shard_map/all_to_all | solution.py:54
  116.8 10.2 %all-to-all-start = ((bf16[256,16,176]{0,2,1:T(8,128)(2,1)}), bf16[256,16,176]{0,2,1:T(8,128)(2,1)S(1)}, u32[]{:S(2)}, u32[]{:S(2)}) async-start(bf16[256,16,176]{0,2,1:T(8,128)(2,1)} %bitcast.3), calls=%async_computation | async-start | bytes 2883584 | tf_op jit(solution)/shard_map/all_to_all | solution.py:53
  127.0 0.9 constant_dynamic-slice_fusion
  128.0 1.3 copy.41
  129.3 78.8 %all-to-all-done = bf16[256,16,176]{0,2,1:T(8,128)(2,1)S(1)} async-done(((bf16[256,16,176]{0,2,1:T(8,128)(2,1)}), bf16[256,16,176]{0,2,1:T(8,128)(2,1)S(1)}, u32[]{:S(2)}, u32[]{:S(2)}) %all-to-all-start) | async-done | bytes 1441824 | tf_op jit(solution)/shard_map/all_to_all | solution.py:53
  208.1 0.0 copy-start.1
  208.1 1.3 copy.40
  209.4 7.2 %all-gather.2.cloned.1.call-done = bf16[512,4096]{0,1:T(8,128)(2,1)} async-done(((bf16[512,256]{0,1:T(8,128)(2,1)}), bf16[512,4096]{0,1:T(8,128)(2,1)}) %all-gather.2.cloned.1.call-update) | async-done | bytes 4194320 | tf_op jit(solution)/shard_map/all_gather | solution.py:57
  216.6 0.0 copy-done.1
  216.6 0.0 copy-start
  216.6 0.0 copy-start.2
  216.6 3.3 fusion.1
  219.8 0.2 copy-done
  220.0 0.4 copy-done.2
  220.4 0.9 fusion
  221.4 0.3 fusion.14
  221.6 0.5 fusion.12
  222.1 1.9 stack.2
  224.0 8.6 %all-to-all-start.3 = ((bf16[16,176,512]{2,1,0:T(8,128)(2,1)}), bf16[16,176,512]{2,1,0:T(8,128)(2,1)S(1)}, u32[]{:S(2)}, u32[]{:S(2)}) async-start(bf16[16,176,512]{2,1,0:T(8,128)(2,1)} %stack.2), calls=%async_computation.3 | async-start | bytes 5767168 | tf_op jit(solution)/shard_map/all_to_all | solution.py:71
  232.6 2.5 copy.35
  235.1 119.6 %all-to-all-done.3 = bf16[16,176,512]{2,1,0:T(8,128)(2,1)S(1)} async-done(((bf16[16,176,512]{2,1,0:T(8,128)(2,1)}), bf16[16,176,512]{2,1,0:T(8,128)(2,1)S(1)}, u32[]{:S(2)}, u32[]{:S(2)}) %all-to-all-start.3) | async-done | bytes 2883616 | tf_op jit(solution)/shard_map/all_to_all | solution.py:71
  354.7 2.3 convolution_bitcast_fusion
  357.0 0.0 copy-start.4
  357.0 13.0 %all_to_all.60 = f32[4,512,64]{1,2,0:T(8,128)S(1)} all-to-all(f32[4,512,64]{1,2,0:T(8,128)S(1)} %convolution_bitcast_fusion), channel_id=1, replica_groups=mesh['ra'=16,'cb'=4,'dp'=8] {'cb'}, dimensions={0} | all-to-all | bytes 1048576 | tf_op jit(solution)/shard_map/all_to_all | solution.py:29
  370.1 0.7 broadcast_in_dim.7
  370.8 12.9 %all-to-all-start.5 = ((f32[64,1,512]{2,1,0:T(1,128)}), f32[64,1,512]{2,1,0:T(1,128)S(1)}, u32[]{:S(2)}, u32[]{:S(2)}) async-start(f32[64,1,512]{2,1,0:T(1,128)} %broadcast_in_dim.7), calls=%async_computation.5 | async-start | bytes 262144 | tf_op jit(solution)/shard_map/all_to_all | solution.py:12
  383.7 0.1 convert_element_type.15
  383.7 0.0 copy-done.4
  383.8 0.1 dynamic_slice.15
  383.8 16.1 %all-to-all-done.5 = f32[64,1,512]{2,1,0:T(1,128)S(1)} async-done(((f32[64,1,512]{2,1,0:T(1,128)}), f32[64,1,512]{2,1,0:T(1,128)S(1)}, u32[]{:S(2)}, u32[]{:S(2)}) %all-to-all-start.5) | async-done | bytes 131104 | tf_op jit(solution)/shard_map/all_to_all | solution.py:12
  400.0 0.1 reduce_sum.49
  400.1 0.1 fusion.13
  400.2 12.3 %all_gather.7 = bf16[512,256]{0,1:T(8,128)(2,1)S(1)} all-gather(bf16[512,64]{0,1:T(8,128)(2,1)S(1)} %fusion.13), channel_id=1, replica_groups=mesh['ra'=16,'cb'=4,'dp'=8] {'cb'}, dimensions={1}, use_global_device_ids=true | all-gather | bytes 327680 | tf_op jit(solution)/shard_map/all_gather | solution.py:87
  412.4 0.8 copy.37
  (5 shorter events, 0.1 us)
Async XLA Ops:
  9.7 27.8 %all-to-all-start.1 = ((f32[16,1,512]{2,1,0:T(1,128)}), f32[16,1,512]{2,1,0:T(1,128)S(1)}, u32[]{:S(2)}, u32[]{:S(2)}) async-start(f32[16,1,512]{2,1,0:T(1,128)} %broadcast_in_dim.6), calls=%async_computation.1 | async-start | bytes 65536 | tf_op jit(solution)/shard_map/all_to_all | solution.py:12
  37.5 4.6 %copy-start.3 = (bf16[256,2816]{1,0:T(8,128)(2,1)S(1)}, bf16[256,2816]{1,0:T(8,128)(2,1)}, u32[]{:S(2)}) copy-start(bf16[256,2816]{1,0:T(8,128)(2,1)} %param.10) | copy-start | bytes 4325380
  37.5 79.2 %all-to-all-start.2 = ((bf16[256,16,176]{0,2,1:T(8,128)(2,1)}), bf16[256,16,176]{0,2,1:T(8,128)(2,1)S(1)}, u32[]{:S(2)}, u32[]{:S(2)}) async-start(bf16[256,16,176]{0,2,1:T(8,128)(2,1)} %bitcast.9), calls=%async_computation.2 | async-start | bytes 2883584 | tf_op jit(solution)/shard_map/all_to_all | solution.py:54
  41.4 175.2 %all-gather.2.cloned.1.call-start = ((), (), s32[]{:S(2)}) async-start(), calls=%async_computation.6 | async-start | bytes 4456448 | tf_op jit(solution)/shard_map/all_gather | solution.py:57
  116.8 91.3 %all-to-all-start = ((bf16[256,16,176]{0,2,1:T(8,128)(2,1)}), bf16[256,16,176]{0,2,1:T(8,128)(2,1)S(1)}, u32[]{:S(2)}, u32[]{:S(2)}) async-start(bf16[256,16,176]{0,2,1:T(8,128)(2,1)} %bitcast.3), calls=%async_computation | async-start | bytes 2883584 | tf_op jit(solution)/shard_map/all_to_all | solution.py:53
  208.1 8.5 %copy-start.1 = (bf16[16,22,8,256]{3,2,0,1:T(8,128)(2,1)S(1)}, bf16[16,22,8,256]{3,2,0,1:T(8,128)(2,1)}, u32[]{:S(2)}) copy-start(bf16[16,22,8,256]{3,2,0,1:T(8,128)(2,1)} %copy.41) | copy-start | bytes 4325380
  216.6 3.4 copy-start
  216.6 3.9 copy-start.2
  224.0 130.7 %all-to-all-start.3 = ((bf16[16,176,512]{2,1,0:T(8,128)(2,1)}), bf16[16,176,512]{2,1,0:T(8,128)(2,1)S(1)}, u32[]{:S(2)}, u32[]{:S(2)}) async-start(bf16[16,176,512]{2,1,0:T(8,128)(2,1)} %stack.2), calls=%async_computation.3 | async-start | bytes 5767168 | tf_op jit(solution)/shard_map/all_to_all | solution.py:71
  357.0 26.8 %copy-start.4 = (f32[256]{0:T(256)S(1)}, f32[256]{0:T(256)}, u32[]{:S(2)}) copy-start(f32[256]{0:T(256)} %param.15) | copy-start | bytes 3076
  370.8 29.1 %all-to-all-start.5 = ((f32[64,1,512]{2,1,0:T(1,128)}), f32[64,1,512]{2,1,0:T(1,128)S(1)}, u32[]{:S(2)}, u32[]{:S(2)}) async-start(f32[64,1,512]{2,1,0:T(1,128)} %broadcast_in_dim.7), calls=%async_computation.5 | async-start | bytes 262144 | tf_op jit(solution)/shard_map/all_to_all | solution.py:12
Sparse Core Ops, SparseCore 0:
  44.3 172.2 all-gather.1
